TPU v7x, 32 devices: a whole 2x2x4 slice. The times are simulated.
32 devices in a mesh: kv: 16 (over z, y, x), tp: 2 (over core).
Axes of the slice: x: 2, y: 2, z: 4, core: 2. Of those that a mesh axis runs over, the one named last changes fastest.
Arguments:
- tokens: bfloat16 [16, 4096], P(None, 'kv'), may hold values from -32 to 32
- attn_gain: float32 [4096], P('kv'), may hold values from 0.1 to 1.9
- w_query: bfloat16 [4096, 4096], P('kv', 'tp'), may hold values from -0.09375 to 0.09375
- w_key: bfloat16 [4096, 4096], P('kv', 'tp'), may hold values from -0.09375 to 0.09375
- w_value: bfloat16 [4096, 4096], P('kv', 'tp'), may hold values from -0.09375 to 0.09375
- key_cache: bfloat16 [16, 2048, 32, 128], P(None, 'kv', 'tp'), may hold values from -128 to 128
- value_cache: bfloat16 [16, 2048, 32, 128], P(None, 'kv', 'tp'), may hold values from -6 to 6
- lengths: int32 [16], replicated, may hold values from 1 to 2048, as said below
- mix_weight: float32 [32], P('tp'), may hold values from 0.3 to 0.8
- head_gain: float32 [128], replicated, may hold values from 0.1 to 1.9
- w_out: bfloat16 [4096, 4096], P('tp', 'kv'), may hold values from -0.09375 to 0.09375
- mixer_gain: float32 [4096], P('kv'), may hold values from 0.1 to 1.9
- w_gate: bfloat16 [4096, 11264], P('kv', 'tp'), may hold values from -0.09375 to 0.09375
- w_up: bfloat16 [4096, 11264], P('kv', 'tp'), may hold values from -0.09375 to 0.09375
- w_down: bfloat16 [11264, 4096], P('tp', 'kv'), may hold values from -0.0546875 to 0.0546875
Outputs:
- layer_out: bfloat16 [16, 4096], P(None, 'kv')
Inputs may be any that keep to these rules, and one draw needn't show every extreme that they name: `lengths`: one sequence has exactly 2048 live positions; four or more sequences, a quarter of them or more, have 4 or fewer.
All inputs are finite; a program needn't handle non-finite values.
Results may differ from a plain program's by a relative error of at most 0.017.
Values may be sent and summed in bfloat16 or wider, within the bound.
A program may use at most 64 MiB of HBM per device.

v0:
```python
import jax
import jax.numpy as jnp
from jax import lax
from jax.sharding import PartitionSpec as P

EPS = 1e-06
FLOOR_SCORE = -1e30


def joined(array, axis, combine):
    everything = jax.tree.map(
        lambda part, kind: lax.all_gather(part.astype(kind), axis),
        array,
        (jnp.bfloat16, jnp.bfloat16, jnp.bfloat16),
    )

    def take(k):
        return jax.tree.map(lambda part, own: part[k].astype(own.dtype), everything, array)

    return lax.fori_loop(
        1, lax.axis_size(axis), lambda k, so_far: combine(so_far, take(k)), take(0)
    )


def combine_parts(first_part, second_part):
    peak_first, totals_first, values_first = first_part
    peak_second, totals_second, values_second = second_part
    peak_score = jnp.maximum(peak_first, peak_second)
    rescale_first = jnp.exp(peak_first - peak_score)
    rescale_second = jnp.exp(peak_second - peak_score)
    return (
        peak_score,
        totals_first * rescale_first + totals_second * rescale_second,
        values_first * rescale_first[..., None] + values_second * rescale_second[..., None],
    )


def local(
    tokens,
    attn_gain,
    w_query,
    w_key,
    w_value,
    key_cache,
    value_cache,
    lengths,
    mix_weight,
    head_gain,
    w_out,
    mixer_gain,
    w_gate,
    w_up,
    w_down,
):
    seq_count = tokens.shape[0]
    head_count = mix_weight.shape[0]
    span_len = key_cache.shape[1]
    head_dim = key_cache.shape[3] // 2
    value_dim = value_cache.shape[3]
    model_width = tokens.shape[1] * lax.axis_size("kv")
    tokens_float = tokens.astype(jnp.float32)
    scaled = (tokens_float * attn_gain).astype(jnp.bfloat16)
    squares, query_sum, key_sum, value_sum = lax.psum(
        (
            jnp.sum(tokens_float * tokens_float, axis=1),
            jnp.dot(scaled, w_query, preferred_element_type=jnp.float32),
            jnp.dot(scaled, w_key, preferred_element_type=jnp.float32),
            jnp.dot(scaled, w_value, preferred_element_type=jnp.float32),
        ),
        "kv",
    )
    inverse = lax.rsqrt(squares / model_width + EPS)[:, None]
    queries = (inverse * query_sum).astype(jnp.bfloat16).reshape(seq_count, head_count, 2, head_dim)
    key_new = (inverse * key_sum).astype(jnp.bfloat16).reshape(seq_count, head_count, 2, head_dim)
    value_new = (inverse * value_sum).astype(jnp.bfloat16).reshape(seq_count, head_count, value_dim)
    logit_scale = head_dim ** (-0.5)
    cached_keys = key_cache.reshape(seq_count, span_len, head_count, 2, head_dim)
    score_matrix = (
        jnp.einsum("bhmd,bphmd->bhmp", queries, cached_keys, preferred_element_type=jnp.float32)
        * logit_scale
    )
    own_score = (
        jnp.sum(queries.astype(jnp.float32) * key_new.astype(jnp.float32), axis=3) * logit_scale
    )
    positions = lax.axis_index("kv") * span_len + jnp.arange(span_len, dtype=jnp.int32)
    visible = (positions[None, :] < lengths[:, None])[:, None, None, :]
    local_peak = jnp.max(jnp.where(visible, score_matrix, FLOOR_SCORE), axis=3)
    weights = jnp.where(visible, jnp.exp(score_matrix - local_peak[..., None]), 0.0)
    local_values = jnp.einsum(
        "bhmp,bphv->bhmv",
        weights.astype(jnp.bfloat16),
        value_cache,
        preferred_element_type=jnp.float32,
    )
    peak_score, totals, accumulated = joined(
        (local_peak, jnp.sum(weights, axis=3), local_values), "kv", combine_parts
    )
    final_peak = jnp.maximum(peak_score, own_score)
    rescale = jnp.exp(peak_score - final_peak)
    own_weight = jnp.exp(own_score - final_peak)
    own_rounded = lax.optimization_barrier(own_weight.astype(jnp.bfloat16)).astype(jnp.float32)
    totals = totals * rescale + own_weight
    accumulated = (
        accumulated * rescale[..., None]
        + own_rounded[..., None] * value_new.astype(jnp.float32)[:, :, None, :]
    )
    mixture = (
        accumulated[:, :, 0] / totals[:, :, 0, None]
        - mix_weight[None, :, None] * accumulated[:, :, 1] / totals[:, :, 1, None]
    )
    head_scale = lax.rsqrt(jnp.mean(mixture * mixture, axis=2, keepdims=True) + EPS)
    attended = (mixture * head_scale * head_gain).astype(jnp.bfloat16)
    attended = attended.reshape(seq_count, head_count * value_dim)
    attention_contribution = lax.psum(
        jnp.dot(attended, w_out, preferred_element_type=jnp.float32).astype(jnp.bfloat16), "tp"
    ).astype(jnp.float32)
    residual = (tokens_float + attention_contribution).astype(jnp.bfloat16)
    residual_f = residual.astype(jnp.float32)
    scaled_mix = (residual_f * mixer_gain).astype(jnp.bfloat16)
    squares_mix = jnp.sum(residual_f * residual_f, axis=1)
    gate_part = jnp.dot(scaled_mix, w_gate, preferred_element_type=jnp.float32)
    up_part = jnp.dot(scaled_mix, w_up, preferred_element_type=jnp.float32)
    squares_all, gate_sum, up_sum = lax.psum((squares_mix, gate_part, up_part), "kv")
    reciprocal_mixture = lax.rsqrt(squares_all / model_width + EPS)[:, None]
    hidden = (jax.nn.silu(reciprocal_mixture * gate_sum) * (reciprocal_mixture * up_sum)).astype(
        jnp.bfloat16
    )
    down_part = jnp.dot(hidden, w_down, preferred_element_type=jnp.float32)
    mixer_term = lax.psum(down_part.astype(jnp.bfloat16), "tp").astype(jnp.float32)
    return (residual_f + mixer_term).astype(jnp.bfloat16)


def solution(mesh):
    return jax.shard_map(
        local,
        mesh=mesh,
        in_specs=(
            P(None, "kv"),
            P("kv"),
            P("kv", "tp"),
            P("kv", "tp"),
            P("kv", "tp"),
            P(None, "kv", "tp", None),
            P(None, "kv", "tp", None),
            P(),
            P("tp"),
            P(),
            P("tp", "kv"),
            P("kv"),
            P("kv", "tp"),
            P("kv", "tp"),
            P("tp", "kv"),
        ),
        out_specs=P(None, "kv"),
        check_vma=False,
    )
```

profile of v0, /device:TPU:25, one launch (start us, length us, event | category | flops | bytes accessed | tf_op | source)
XLA Modules:
  0.0 418.9 jit_solution(10726314257851681850)
XLA Ops:
  6.5 2.3 fusion.35
  8.9 2.1 fusion.33
  11.0 2.2 fusion.31
  13.4 26.9 %psum.63 = f32[16]{0:T(128)S(1)} all-reduce(f32[16]{0:T(128)S(1)} %fusion.20), channel_id=1, replica_groups=mesh['kv'=16,'tp'=2] {'kv'}, use_global_device_ids=true, to_apply=%region_1.0 | all-reduce | flops 16 | bytes 128 | tf_op jit(solution)/shard_map/psum | solution.py:63
  40.3 12.9 %copy.59 = bf16[16,128,16,128]{1,3,2,0:T(8,128)(2,1)} copy(bf16[16,128,16,128]{3,2,1,0:T(8,128)(2,1)} %param.22) | data formatting | bytes 16777216 | tf_op args[5]
  53.2 68.1 %all-reduce.7.cloned.1.call-done = (f32[16,2048]{1,0:T(8,128)}, f32[16,2048]{1,0:T(8,128)}, f32[16,2048]{1,0:T(8,128)}) async-done(((f32[16,2048]{1,0:T(8,128)}, f32[16,2048]{1,0:T(8,128)}, f32[16,2048]{1,0:T(8,128)}), (f32[16,2048]{1,0:T(8,128)}, f32[16,2048]{1,0:T(8,128)}, f32[16,2048]{1,0:T(8,128)})) %all-reduce.7.cloned.1.call-update) | async-done | bytes 393232 | tf_op jit(solution)/shard_map/psum | solution.py:63
  121.3 1.8 fusion.14
  124.0 5.7 %fusion.42 = f32[16,16,2,1,128]{4,3,2,1,0:T(1,128)S(1)} fusion(bf16[16,16,2,64,1]{3,4,2,1,0:T(2,128)(2,1)} %reshape.124, bf16[16,128,16,2,64]{1,4,3,2,0:T(8,128)(2,1)} %bitcast.82), kind=kOutput, calls=%fused_computation.77 | convolution fusion | flops 8388608 | bytes 8716288 | tf_op jit(solution)/shard_map/bhmd,bphmd->bhmp/dot_general | solution.py:79
  130.2 5.7 %fusion.5 = bf16[16,16,2,128]{3,2,1,0:T(2,128)(2,1)S(1)} fusion(bf16[16,128,16,128]{3,2,1,0:T(8,128)(2,1)} %param.23, pred[16,128]{1,0:T(8,128)(4,1)S(1)} %broadcast_compare_fusion, f32[16,16,2,128]{3,2,1,0:T(2,128)S(1)} %bitcast.86, f32[16,16,2]{2,1,0:T(8,128)S(1)} %select_reduce_fusion), kind=kOutput, calls=%fused_computation.12 | convolution fusion | flops 17104896 | bytes 8785920 | tf_op jit(solution)/shard_map/bhmp,bphv->bhmv/dot_general | solution.py:89
  138.3 1.1 reshape.107
  139.4 1.6 copy.79
  141.0 1.9 multiply_reduce_fusion
  142.9 1.7 copy.68
  145.5 28.2 %all-gather.1 = bf16[256,16,2]{1,2,0:T(2,128)(2,1)} all-gather(bf16[16,16,2]{1,2,0:T(2,128)(2,1)S(1)} %copy.63), channel_id=3, replica_groups=mesh['kv'=16,'tp'=2] {'kv'}, dimensions={0}, use_global_device_ids=true | all-gather | bytes 17408 | tf_op jit(solution)/shard_map/all_gather | solution.py:12
  173.7 33.0 %all-gather = bf16[256,16,2]{1,2,0:T(2,128)(2,1)} all-gather(bf16[16,16,2]{1,2,0:T(2,128)(2,1)S(1)} %copy.61), channel_id=2, replica_groups=mesh['kv'=16,'tp'=2] {'kv'}, dimensions={0}, use_global_device_ids=true | all-gather | bytes 17408 | tf_op jit(solution)/shard_map/all_gather | solution.py:12
  206.7 1.3 slice_convert_fusion.1
  208.0 1.3 slice_convert_fusion.2
  209.3 0.9 slice_convert_fusion
  210.4 53.9 %while.19 = (s32[]{:T(128)}, f32[16,16,2]{1,2,0:T(2,128)}, f32[16,16,2]{1,2,0:T(2,128)}, f32[16,16,2,128]{3,2,1,0:T(2,128)S(1)}, bf16[16,16,16,2]{2,3,1,0:T(2,12...) while((s32[]{:T(128)}, f32[16,16,2]{1,2,0:T(2,128)}, ...), condition=%wide.region_6.7_spmd, body=%wide.region_5.0_spmd.sunk | while | flops 266245 | bytes 944271 | solution.py:20
  210.4 1.4 fusion.54
  211.8 0.9 constant_dynamic-slice_fusion.2
  213.0 0.9 fusion.55
  214.0 1.4 fusion.54
  216.6 0.9 fusion.55
  217.6 1.4 fusion.54
  219.0 0.9 constant_dynamic-slice_fusion.2
  220.2 0.9 fusion.55
  221.2 1.4 fusion.54
  223.8 0.9 fusion.55
  224.8 1.4 fusion.54
  226.2 0.9 constant_dynamic-slice_fusion.2
  227.4 0.9 fusion.55
  228.4 1.4 fusion.54
  231.0 0.9 fusion.55
  232.0 1.4 fusion.54
  233.4 0.9 constant_dynamic-slice_fusion.2
  234.6 0.9 fusion.55
  235.6 1.4 fusion.54
  237.0 0.9 constant_dynamic-slice_fusion.2
  238.2 0.9 fusion.55
  239.2 1.4 fusion.54
  240.6 0.9 constant_dynamic-slice_fusion.2
  241.8 0.9 fusion.55
  242.7 1.4 fusion.54
  245.4 0.9 fusion.55
  246.3 1.4 fusion.54
  249.0 0.9 fusion.55
  249.9 1.4 fusion.54
  252.6 0.9 fusion.55
  253.5 1.4 fusion.54
  256.2 0.9 fusion.55
  257.1 1.4 fusion.54
  259.8 0.9 fusion.55
  260.7 1.4 fusion.54
  263.4 0.9 fusion.55
  265.5 1.5 multiply_add_fusion
  268.7 1.6 convolution_convert_fusion.1
  270.4 18.9 %psum.67 = bf16[16,256]{1,0:T(8,128)(2,1)S(1)} all-reduce(bf16[16,256]{1,0:T(8,128)(2,1)S(1)} %convolution_convert_fusion.1), channel_id=1, replica_groups=mesh['kv'=16,'tp'=2] {'tp'}, use_global_device_ids=true, to_apply=%region_11.12 | all-reduce | flops 4096 | bytes 16384 | tf_op jit(solution)/shard_map/psum | solution.py:114
  289.4 1.2 fusion.29
  291.2 1.2 fusion.27
  292.4 30.5 %psum.68 = f32[16]{0:T(128)S(1)} all-reduce(f32[16]{0:T(128)S(1)} %get-tuple-element.230), channel_id=1, replica_groups=mesh['kv'=16,'tp'=2] {'kv'}, use_global_device_ids=true, to_apply=%region_13.14 | all-reduce | flops 16 | bytes 128 | tf_op jit(solution)/shard_map/psum | solution.py:123
  323.0 81.2 %all-reduce.5.cloned.1.call-done = (f32[16,5632]{1,0:T(8,128)}, f32[16,5632]{1,0:T(8,128)}) async-done(((f32[16,5632]{1,0:T(8,128)}, f32[16,5632]{1,0:T(8,128)}), (f32[16,5632]{1,0:T(8,128)}, f32[16,5632]{1,0:T(8,128)})) %all-reduce.5.cloned.1.call-update) | async-done | bytes 720912 | tf_op jit(solution)/shard_map/psum | solution.py:123
  404.1 2.6 convolution_convert_fusion
  406.7 5.1 %psum.71 = bf16[16,256]{1,0:T(8,128)(2,1)S(1)} all-reduce(bf16[16,256]{1,0:T(8,128)(2,1)S(1)} %convolution_convert_fusion), channel_id=1, replica_groups=mesh['kv'=16,'tp'=2] {'tp'}, use_global_device_ids=true, to_apply=%region_16.17 | all-reduce | flops 4096 | bytes 16384 | tf_op jit(solution)/shard_map/psum | solution.py:129
  (90 shorter events, 22.4 us)
Async XLA Ops:
  6.5 282.8 %copy-start = (bf16[256,5632]{1,0:T(8,128)(2,1)S(1)}, bf16[256,5632]{1,0:T(8,128)(2,1)}, u32[]{:S(2)}) copy-start(bf16[256,5632]{1,0:T(8,128)(2,1)} %param.29) | copy-start | bytes 8650756
  6.5 6.7 %copy-start.2 = (bf16[16,256]{1,0:T(8,128)(2,1)S(1)}, bf16[16,256]{1,0:T(8,128)(2,1)}, u32[]{:S(2)}) copy-start(bf16[16,256]{1,0:T(8,128)(2,1)} %param.17) | copy-start | bytes 24580
  6.5 114.8 %all-reduce.7.cloned.1.call-start = ((), (), s32[]{:S(2)}) async-start(), calls=%async_computation.2 | async-start | bytes 786432 | tf_op jit(solution)/shard_map/psum | solution.py:63
  13.2 196.1 %all-gather.5.cloned.1.call-start = ((), (), s32[]{:S(2)}) async-start(), calls=%async_computation | async-start | bytes 2228224 | tf_op jit(solution)/shard_map/all_gather | solution.py:12
  40.3 12.9 %copy-start.7 = (s32[16]{0:T(128)S(1)}, s32[16]{0:T(128)}, u32[]{:S(2)}) copy-start(s32[16]{0:T(128)} %param.24) | copy-start | bytes 196
  130.1 6.5 %copy-start.5 = (f32[16]{0:T(128)S(1)}, f32[16]{0:T(128)}, u32[]{:S(2)}) copy-start(f32[16]{0:T(128)} %param.25) | copy-start | bytes 196
  130.2 6.5 %copy-start.6 = (f32[128]{0:T(128)S(1)}, f32[128]{0:T(128)}, u32[]{:S(2)}) copy-start(f32[128]{0:T(128)} %param.26) | copy-start | bytes 1540
  136.6 267.5 %all-reduce.5.cloned.1.call-start = ((), (), s32[]{:S(2)}) async-start(), calls=%async_computation.1 | async-start | bytes 1441792 | tf_op jit(solution)/shard_map/psum | solution.py:123
  264.3 24.9 %copy-start.3 = (bf16[16,256]{1,0:T(8,128)(2,1)S(1)}, bf16[16,256]{1,0:T(8,128)(2,1)}, u32[]{:S(2)}) copy-start(bf16[16,256]{1,0:T(8,128)(2,1)} %param.17) | copy-start | bytes 24580
  264.3 25.0 %copy-start.4 = (f32[256]{0:T(256)S(1)}, f32[256]{0:T(256)}, u32[]{:S(2)}) copy-start(f32[256]{0:T(256)} %param.28) | copy-start | bytes 3076
  289.2 1.9 copy-start.1
Sparse Core Ops, SparseCore 0:
  13.3 107.9 all-reduce.6
  136.7 61.0 all-gather.4
  292.5 111.5 all-reduce.4
where the time goes:
time: 423 us; the launch traced here: 419 us
  waiting for transfers between devices  149 us (35%)
  blocking collectives  142 us (34%)
  other arithmetic  47.2 us (11%)
  local copies, waits for them, and re-layouts  41.3 us (10%)
  matrix products  24.8 us (6%)
  between operations  13.3 us (3%)
    psum x1, waiting for transfers between devices, local(): lax.psum((squares_mix, gate_part, up_part), 'kv')  81.2 us
    psum x1, waiting for transfers between devices, local(): lax.psum((jnp.sum(tokens_float * tokens_float, axis=1), jnp.dot(scaled, w...  68.1 us
    all_gather x2, blocking collectives, joined(): lax.all_gather(part.astype(kind), axis)  61.2 us
    psum x1, blocking collectives, local(): lax.psum((squares_mix, gate_part, up_part), 'kv')  30.5 us
    psum x1, blocking collectives, local(): lax.psum((jnp.sum(tokens_float * tokens_float, axis=1), jnp.dot(scaled, w...  26.9 us
    add x15, other arithmetic, combine_parts(): totals_first * rescale_first + totals_second * rescale_second  21 us
    psum x1, blocking collectives, local(): lax.psum(jnp.dot(attended, w_out, preferred_element_type=jnp.float32).ast...  18.9 us
    unnamed x18, local copies, waits for them, and re-layouts  15.1 us
  transfers between devices with their start and end apart: 3, of which 2 were waited for; matrix products, arithmetic and copies ran while one was open for 6% of the time, Pallas kernels for 0%

commit v1 on v0

v1 whole, which is shorter than its diff:
```python
import functools

import jax
import jax.numpy as jnp
from jax import lax
from jax.experimental import pallas as pl
from jax.experimental.pallas import tpu as pltpu
from jax.sharding import PartitionSpec as P

EPS = 1e-06
FLOOR_SCORE = -1e30
LANES = 128
F32 = jnp.float32
BF16 = jnp.bfloat16
VMEM = pl.BlockSpec(memory_space=pltpu.VMEM)
SMEM = pl.BlockSpec(memory_space=pltpu.SMEM)
ANY = pl.BlockSpec(memory_space=pl.ANY)


def greet(n, me, others=()):
    barrier = pltpu.get_barrier_semaphore()
    for i in range(1, n):
        pl.semaphore_signal(
            barrier,
            inc=1,
            device_id={"kv": lax.rem(me + i, n)},
            device_id_type=pl.DeviceIdType.MESH,
        )
    for other in others:
        pl.semaphore_signal(
            barrier, inc=1, device_id={"tp": other}, device_id_type=pl.DeviceIdType.MESH
        )
    return barrier, n - 1 + len(others)


def landed(buf, recv, k):
    pltpu.make_async_copy(buf.at[k], buf.at[k], recv.at[k]).wait()


def remote(src, dst, send_sem, recv_sem, target):
    return pltpu.make_async_remote_copy(
        src_ref=src,
        dst_ref=dst,
        send_sem=send_sem,
        recv_sem=recv_sem,
        device_id=target,
        device_id_type=pl.DeviceIdType.MESH,
    )


def each_owner(n, owners, me, body):
    for i in range(owners):
        if owners == n:
            if i > 0:
                body(lax.rem(me + i, n))
        else:
            o = lax.rem(me + i, owners)
            pl.when(o != me)(functools.partial(body, o))


def when_owner(n, owners, me, body):
    if owners == n:
        body()
    else:
        pl.when(me < owners)(body)


def project_kernel(
    n, heads, width, tokens, gain, wq, wk, wv, q_out, own_out,
    sbuf, rbuf, gsrc, gbuf, send, recv,
):
    me = lax.axis_index("kv")
    barrier, count = greet(n, me)
    tokens_f = tokens[...].astype(F32)
    scaled = (tokens_f * gain[...]).astype(BF16)
    squares = jnp.sum(tokens_f * tokens_f, axis=1, keepdims=True)
    squares = jnp.broadcast_to(squares, (tokens.shape[0], LANES))
    for j, w in enumerate((wq, wk, wv)):
        part = jnp.dot(scaled, w[...], preferred_element_type=F32)
        for h in range(heads):
            sbuf[h, j] = part[:, h * LANES : (h + 1) * LANES]
    for h in range(heads):
        sbuf[h, 3] = squares
    pl.semaphore_wait(barrier, count)

    def reduce_copy(o):
        return remote(sbuf.at[o], rbuf.at[me], send.at[0, o], recv.at[0, me], {"kv": o})

    def gather_copy(o):
        return remote(gsrc, gbuf.at[me], send.at[1, o], recv.at[1, me], {"kv": o})

    each_owner(n, heads, me, lambda o: reduce_copy(o).start())

    def own():
        rbuf[me] = sbuf[me]
        for i in range(1, n):
            landed(rbuf, recv.at[0], lax.rem(me + n - i, n))
        total = rbuf[0]
        for k in range(1, n):
            total = total + rbuf[k]
        inverse = lax.rsqrt(total[3] / width + EPS)
        for j in range(3):
            own_out[j] = (inverse * total[j]).astype(BF16)
        gsrc[...] = (inverse * total[0]).astype(BF16)
        for i in range(1, n):
            gather_copy(lax.rem(me + i, n)).start()
        gbuf[me] = (inverse * total[0]).astype(BF16)

    when_owner(n, heads, me, own)
    each_owner(n, heads, me, lambda o: landed(gbuf, recv.at[1], o))
    q_out[...] = gbuf[...]
    each_owner(n, heads, me, lambda o: reduce_copy(o).wait_send())

    def drain():
        for i in range(1, n):
            gather_copy(lax.rem(me + i, n)).wait_send()

    when_owner(n, heads, me, drain)


def attend_kernel(heads, scale, info, q_ref, k_ref, v_ref, value_out, lse_out):
    b = pl.program_id(0)
    live = info[1, b]
    rows = 2 * heads

    @pl.when(live > 0)
    def _():
        q = q_ref[0]
        lane = lax.broadcasted_iota(jnp.int32, q.shape, 1)
        half = q.shape[1] // 2
        zero = jnp.zeros_like(q)
        queries = jnp.concatenate(
            [jnp.where(lane < half, q, zero), jnp.where(lane >= half, q, zero)], axis=0
        )
        keys = k_ref[0].reshape(-1, k_ref.shape[3])
        values = v_ref[0].reshape(-1, v_ref.shape[3])
        scores = lax.dot_general(
            queries, keys, (((1,), (1,)), ((), ())), preferred_element_type=F32
        )
        column = lax.broadcasted_iota(jnp.int32, scores.shape, 1)
        row = lax.broadcasted_iota(jnp.int32, scores.shape, 0)
        visible = (lax.rem(column, heads) == lax.rem(row, heads)) & (column < live * heads)
        scores = jnp.where(visible, scores * scale, FLOOR_SCORE)
        peak = jnp.max(scores, axis=1, keepdims=True)
        weights = jnp.where(visible, jnp.exp(scores - peak), 0.0)
        totals = jnp.sum(weights, axis=1, keepdims=True)
        position = lax.broadcasted_iota(jnp.int32, values.shape, 0)
        values = jnp.where(position < live * heads, values, jnp.zeros_like(values))
        summed = jnp.dot(weights.astype(BF16), values, preferred_element_type=F32)
        value_out[0] = (summed / totals).astype(BF16)
        lse_out[0] = jnp.broadcast_to(peak + jnp.log(totals), (rows, LANES))

    @pl.when(live <= 0)
    def _():
        value_out[0] = jnp.zeros(value_out.shape[1:], BF16)
        lse_out[0] = jnp.full((rows, LANES), FLOOR_SCORE, F32)


def finish_kernel(
    n, team, heads, owners, tile, width, scale,
    vals, lses, own_qkv, mix, head_gain, tokens, mixer_gain, w_out, w_gate, w_up, w_down,
    out,
    wo, wg, wu, wd, rvals, rlses, asrc, agat, xsrc, xdst, ssrc, sdst,
    gsrc, gdst, hsrc, hgat, ysrc, ydst, send, recv, tsend, trecv, load,
):
    me = lax.axis_index("kv")
    mate = lax.axis_index("tp")
    mates = [lax.rem(mate + i, team) for i in range(1, team)]
    barrier, count = greet(n, me, mates)
    hidden_width = w_gate.shape[1]
    loads = [
        pltpu.make_async_copy(w_out, wo, load.at[0]),
        pltpu.make_async_copy(w_gate, wg.at[:, pl.ds(0, hidden_width)], load.at[1]),
        pltpu.make_async_copy(w_up, wu.at[:, pl.ds(0, hidden_width)], load.at[2]),
        pltpu.make_async_copy(w_down, wd, load.at[3]),
    ]
    for copy in loads:
        copy.start()
    padded = owners * tile
    if padded > hidden_width:
        for w in (wg, wu):
            w[:, pl.ds(hidden_width, padded - hidden_width)] = jnp.zeros(
                (w.shape[0], padded - hidden_width), BF16
            )
    pl.semaphore_wait(barrier, count)

    def vals_copy(o):
        return remote(vals.at[o], rvals.at[me], send.at[0, o], recv.at[0, me], {"kv": o})

    def lses_copy(o):
        return remote(lses.at[o], rlses.at[me], send.at[1, o], recv.at[1, me], {"kv": o})

    def attended_copy(o):
        return remote(asrc, agat.at[me], send.at[2, o], recv.at[2, me], {"kv": o})

    def start_parts(o):
        lses_copy(o).start()
        vals_copy(o).start()

    each_owner(n, heads, me, start_parts)

    def own_head():
        rvals[me] = vals[me]
        rlses[me] = lses[me]
        q, k, v = (own_qkv[j].astype(F32) for j in range(3))
        product = q * k
        lane = lax.broadcasted_iota(jnp.int32, product.shape, 1)
        half = product.shape[1] // 2
        own_scores = [
            jnp.sum(jnp.where(side, product, 0.0), axis=1, keepdims=True) * scale
            for side in (lane < half, lane >= half)
        ]
        for i in range(1, n):
            landed(rlses, recv.at[1], lax.rem(me + n - i, n))
            landed(rvals, recv.at[0], lax.rem(me + n - i, n))
        normed = []
        for m in range(2):
            own_score = jnp.broadcast_to(own_scores[m], v.shape)
            peak = own_score
            for j in range(n):
                peak = jnp.maximum(peak, rlses[j, m])
            own_weight = jnp.exp(own_score - peak)
            totals = own_weight
            summed = own_weight.astype(BF16).astype(F32) * v
            for j in range(n):
                weight = jnp.exp(rlses[j, m] - peak)
                totals = totals + weight
                summed = summed + weight * rvals[j, m].astype(F32)
            normed.append(summed / totals)
        mixture = normed[0] - mix[0, me] * normed[1]
        head_scale = lax.rsqrt(jnp.mean(mixture * mixture, axis=1, keepdims=True) + EPS)
        attended = (mixture * head_scale * head_gain[...]).astype(BF16)
        asrc[...] = attended
        for i in range(1, n):
            attended_copy(lax.rem(me + i, n)).start()
        agat[me] = attended

    when_owner(n, heads, me, own_head)
    loads[0].wait()
    each_owner(n, heads, me, lambda o: landed(agat, recv.at[2], o))
    attended_all = jnp.concatenate([agat[h] for h in range(heads)], axis=1)
    part = jnp.dot(attended_all, wo[...], preferred_element_type=F32).astype(BF16)
    xsrc[...] = part

    def swap_copy(src, dst, phase, other):
        return remote(
            src, dst.at[mate], tsend.at[phase, other], trecv.at[phase, mate], {"tp": other}
        )

    def team_sum(src, dst, phase):
        for other in mates:
            swap_copy(src, dst, phase, other).start()
        total = src[...].astype(F32)
        for other in mates:
            landed(dst, trecv.at[phase], other)
            total = total + dst[other].astype(F32)
        return total

    residual = (tokens[...].astype(F32) + team_sum(xsrc, xdst, 0)).astype(BF16)
    residual_f = residual.astype(F32)
    scaled_mix = (residual_f * mixer_gain[...]).astype(BF16)
    squares = jnp.sum(residual_f * residual_f, axis=1, keepdims=True)
    ssrc[...] = jnp.broadcast_to(squares, ssrc.shape)

    def squares_copy(o):
        return remote(ssrc, sdst.at[me], send.at[3, o], recv.at[3, me], {"kv": o})

    def gate_copy(o):
        return remote(gsrc.at[o], gdst.at[me], send.at[4, o], recv.at[4, me], {"kv": o})

    def hidden_copy(o):
        return remote(hsrc, hgat.at[me], send.at[5, o], recv.at[5, me], {"kv": o})

    loads[1].wait()
    loads[2].wait()
    each_owner(n, owners, me, lambda o: squares_copy(o).start())
    for i in range(owners):
        o = lax.rem(me + 1 + i, owners)
        columns = pl.ds(pl.multiple_of(o * tile, LANES), tile)
        for j, w in enumerate((wg, wu)):
            gsrc[o, j] = jnp.dot(
                scaled_mix, w[:, columns], preferred_element_type=F32
            ).astype(BF16)
        pl.when(o != me)(lambda: gate_copy(o).start())

    def own_hidden():
        sdst[me] = ssrc[...]
        gdst[me] = gsrc[me]
        for i in range(1, n):
            landed(sdst, recv.at[3], lax.rem(me + n - i, n))
            landed(gdst, recv.at[4], lax.rem(me + n - i, n))
        total = sdst[0]
        for j in range(1, n):
            total = total + sdst[j]
        inverse = lax.rsqrt(total[:, :1] / width + EPS)
        gate = gdst[0, 0].astype(F32)
        up = gdst[0, 1].astype(F32)
        for j in range(1, n):
            gate = gate + gdst[j, 0].astype(F32)
            up = up + gdst[j, 1].astype(F32)
        gate = inverse * gate
        hidden = (gate / (1.0 + jnp.exp(-gate)) * (inverse * up)).astype(BF16)
        hsrc[...] = hidden
        for i in range(1, n):
            hidden_copy(lax.rem(me + i, n)).start()
        hgat[me] = hidden

    when_owner(n, owners, me, own_hidden)
    loads[3].wait()
    each_owner(n, owners, me, lambda o: landed(hgat, recv.at[5], o))
    hidden_all = jnp.concatenate([hgat[o] for o in range(owners)], axis=1)[:, :hidden_width]
    down = jnp.dot(hidden_all, wd[...], preferred_element_type=F32).astype(BF16)
    ysrc[...] = down
    out[...] = (residual_f + team_sum(ysrc, ydst, 1)).astype(BF16)

    each_owner(n, heads, me, lambda o: vals_copy(o).wait_send())
    each_owner(n, heads, me, lambda o: lses_copy(o).wait_send())
    for other in mates:
        swap_copy(xsrc, xdst, 0, other).wait_send()
        swap_copy(ysrc, ydst, 1, other).wait_send()
    each_owner(n, owners, me, lambda o: squares_copy(o).wait_send())
    each_owner(n, owners, me, lambda o: gate_copy(o).wait_send())

    def drain(copy):
        for i in range(1, n):
            copy(lax.rem(me + i, n)).wait_send()

    when_owner(n, heads, me, lambda: drain(attended_copy))
    when_owner(n, owners, me, lambda: drain(hidden_copy))


def local(
    n, team, tokens, attn_gain, w_query, w_key, w_value, key_cache, value_cache, lengths,
    mix_weight, head_gain, w_out, mixer_gain, w_gate, w_up, w_down,
):
    seqs, span_width = tokens.shape
    heads = mix_weight.shape[0]
    span = key_cache.shape[1]
    scale = (key_cache.shape[3] // 2) ** -0.5
    width = span_width * n
    hidden_width = w_gate.shape[1]
    tiles = hidden_width // LANES
    tile = -(-tiles // n)
    owners = -(-tiles // tile)
    tile *= LANES
    remote_params = functools.partial(
        pltpu.CompilerParams, has_side_effects=True, vmem_limit_bytes=60 * 2**20
    )

    queries, own_qkv = pl.pallas_call(
        functools.partial(project_kernel, n, heads, width),
        out_shape=(
            jax.ShapeDtypeStruct((heads, seqs, LANES), BF16),
            jax.ShapeDtypeStruct((3, seqs, LANES), BF16),
        ),
        in_specs=[VMEM] * 5,
        out_specs=(VMEM, VMEM),
        scratch_shapes=[
            pltpu.VMEM((heads, 4, seqs, LANES), F32),
            pltpu.VMEM((n, 4, seqs, LANES), F32),
            pltpu.VMEM((seqs, LANES), BF16),
            pltpu.VMEM((heads, seqs, LANES), BF16),
            pltpu.SemaphoreType.DMA((2, n)),
            pltpu.SemaphoreType.DMA((2, n)),
        ],
        compiler_params=remote_params(collective_id=0),
        name="project",
    )(tokens, attn_gain[None], w_query, w_key, w_value)

    live = lengths - lax.axis_index("kv") * span
    order = jnp.arange(seqs, dtype=jnp.int32)
    seen = (order[None, :] <= order[:, None]) & (live > 0)[None, :]
    fetch = jnp.max(jnp.where(seen, order[None, :], 0), axis=1)
    info = jnp.stack([fetch, live])

    cache_spec = pl.BlockSpec(
        (1, *key_cache.shape[1:]), lambda b, info: (info[0, b], 0, 0, 0)
    )
    part_spec = pl.BlockSpec((1, 2 * heads, LANES), lambda b, info: (b, 0, 0))
    values, lses = pl.pallas_call(
        functools.partial(attend_kernel, heads, scale),
        out_shape=(
            jax.ShapeDtypeStruct((seqs, 2 * heads, LANES), BF16),
            jax.ShapeDtypeStruct((seqs, 2 * heads, LANES), F32),
        ),
        grid_spec=pltpu.PrefetchScalarGridSpec(
            num_scalar_prefetch=1,
            grid=(seqs,),
            in_specs=[
                pl.BlockSpec((1, heads, LANES), lambda b, info: (b, 0, 0)),
                cache_spec,
                cache_spec,
            ],
            out_specs=(part_spec, part_spec),
        ),
        compiler_params=pltpu.CompilerParams(
            dimension_semantics=("arbitrary",), vmem_limit_bytes=60 * 2**20
        ),
        name="attend",
    )(info, queries.transpose(1, 0, 2), key_cache, value_cache)

    def by_head(array):
        return array.reshape(seqs, 2, heads, LANES).transpose(2, 1, 0, 3)

    return pl.pallas_call(
        functools.partial(finish_kernel, n, team, heads, owners, tile, width, scale),
        out_shape=jax.ShapeDtypeStruct((seqs, span_width), BF16),
        in_specs=[VMEM, VMEM, VMEM, SMEM, VMEM, VMEM, VMEM, ANY, ANY, ANY, ANY],
        out_specs=VMEM,
        scratch_shapes=[
            pltpu.VMEM(w_out.shape, BF16),
            pltpu.VMEM((span_width, owners * tile), BF16),
            pltpu.VMEM((span_width, owners * tile), BF16),
            pltpu.VMEM(w_down.shape, BF16),
            pltpu.VMEM((n, 2, seqs, LANES), BF16),
            pltpu.VMEM((n, 2, seqs, LANES), F32),
            pltpu.VMEM((seqs, LANES), BF16),
            pltpu.VMEM((heads, seqs, LANES), BF16),
            pltpu.VMEM((seqs, span_width), BF16),
            pltpu.VMEM((team, seqs, span_width), BF16),
            pltpu.VMEM((seqs, LANES), F32),
            pltpu.VMEM((n, seqs, LANES), F32),
            pltpu.VMEM((owners, 2, seqs, tile), BF16),
            pltpu.VMEM((n, 2, seqs, tile), BF16),
            pltpu.VMEM((seqs, tile), BF16),
            pltpu.VMEM((owners, seqs, tile), BF16),
            pltpu.VMEM((seqs, span_width), BF16),
            pltpu.VMEM((team, seqs, span_width), BF16),
            pltpu.SemaphoreType.DMA((6, n)),
            pltpu.SemaphoreType.DMA((6, n)),
            pltpu.SemaphoreType.DMA((2, team)),
            pltpu.SemaphoreType.DMA((2, team)),
            pltpu.SemaphoreType.DMA((4,)),
        ],
        compiler_params=remote_params(collective_id=1),
        name="finish",
    )(
        by_head(values), by_head(lses), own_qkv, mix_weight[None], head_gain[None],
        tokens, mixer_gain[None], w_out, w_gate, w_up, w_down,
    )


def solution(mesh):
    return jax.shard_map(
        functools.partial(local, mesh.shape["kv"], mesh.shape["tp"]),
        mesh=mesh,
        in_specs=(
            P(None, "kv"),
            P("kv"),
            P("kv", "tp"),
            P("kv", "tp"),
            P("kv", "tp"),
            P(None, "kv", "tp", None),
            P(None, "kv", "tp", None),
            P(),
            P("tp"),
            P(),
            P("tp", "kv"),
            P("kv"),
            P("kv", "tp"),
            P("kv", "tp"),
            P("tp", "kv"),
        ),
        out_specs=P(None, "kv"),
        check_vma=False,
    )
```

time: 423 us -> 95.8 us (0.23)
  waiting for transfers between devices: 149 us -> 0 us
  blocking collectives: 142 us -> 0 us
  Pallas kernels: 0 us -> 86.9 us
  other arithmetic: 47.2 us -> 2.01 us
  local copies, waits for them, and re-layouts: 41.3 us -> 6.18 us
  matrix products: 24.8 us -> 0 us
  between operations: 13.3 us -> 0.02 us
    psum x2 -> x0, waiting for transfers between devices: 149 us -> none  [the longest x1 81.2 us: local(): lax.psum((squares_mix, gate_part, up_part), 'kv')]
    pallas_call x0 -> x3, Pallas kernels: none -> 86.9 us  [the longest x1 54.1 us: local(): pl.pallas_call(functools.partial(finish_kernel, n, team, heads, owners, t...]
    psum x4 -> x0, blocking collectives: 81.3 us -> none  [the longest x1 30.5 us: local(): lax.psum((squares_mix, gate_part, up_part), 'kv')]
    all_gather x2 -> x0, blocking collectives: 61.2 us -> none  [joined(): lax.all_gather(part.astype(kind), axis)]
    add x33 -> x0, other arithmetic: 37 us -> none  [the longest x15 21 us: combine_parts(): totals_first * rescale_first + totals_second * rescale_second]
    dot_general x9 -> x0, matrix products: 24.8 us -> none  [the longest x1 5.74 us: local(): jnp.einsum('bhmd,bphmd->bhmp', queries, cached_keys, preferred_element_ty...]
    unnamed x18 -> x1, local copies, waits for them, and re-layouts: 15.1 us -> 1.3 us
    dynamic_slice x15 -> x0, local copies, waits for them, and re-layouts: 13.7 us -> none  [take(): part[k].astype(own.dtype)]
  transfers between devices with their start and end apart: 3 -> 0, of which waited for: 2 -> 0; matrix products, arithmetic and copies ran while one was open for 6% -> 0% of each run, Pallas kernels for 0% -> 0%
where the time goes in v1:
time: 95.8 us; the launch traced here: 95.1 us
  Pallas kernels  86.9 us (91%)
  local copies, waits for them, and re-layouts  6.18 us (6%)
  other arithmetic  2.01 us (2%)
    pallas_call x1, Pallas kernels, local(): pl.pallas_call(functools.partial(finish_kernel, n, team, heads, owners, t...  54.1 us
    pallas_call x1, Pallas kernels, local(): pl.pallas_call(functools.partial(project_kernel, n, heads, width), out_sh...  23.5 us
    pallas_call x1, Pallas kernels, local(): pl.pallas_call(functools.partial(attend_kernel, heads, scale), out_shape=...  9.32 us
    reshape x2, local copies, waits for them, and re-layouts, by_head(): return array.reshape(seqs, 2, heads, LANES).transpose(2, 1, 0, 3)  3.41 us

profile of v1, /device:TPU:25, one launch (start us, length us, event | category | flops | bytes accessed | tf_op | source)
XLA Modules:
  0.0 95.1 jit_solution(16597027737427355831)
XLA Ops:
  0.0 0.7 subtract_bitcast_fusion
  0.7 0.7 subtract_compare_fusion
  1.3 0.1 select_reduce_fusion
  1.4 0.6 pad_add_fusion.info
  2.0 23.5 %project.1 = (bf16[16,16,128]{2,1,0:T(8,128)(2,1)}, bf16[3,16,128]{2,1,0:T(8,128)(2,1)}) custom-call(bf16[16,256]{1,0:T(8,128)(2,1)} %tokens.3, f32[1,256]{1,0:T(1,128)} %bitcast.23, bf16[256,2048]{1,0:T(8,128)(2,1)} %wq.1, bf16[256,2048]{1,0:T(8,128)(2,1)} %wk.1, bf16[256,2048]{1,0:T(8,128)(2,1)} %wv.1), custom_call_target="tpu_custom_call" | custom-call | tf_op jit(solution)/shard_map/project/pallas_call | solution.py:350
  25.5 1.5 %copy.28 = bf16[16,16,128]{2,0,1:T(8,128)(2,1)} copy(bf16[16,16,128]{2,1,0:T(8,128)(2,1)} %get-tuple-element.9) | data formatting | bytes 131072 | tf_op jit(solution)/shard_map/project/pallas_call | solution.py:350
  26.9 9.3 %attend.1 = (bf16[16,32,128]{2,1,0:T(8,128)(2,1)}, f32[16,32,128]{2,1,0:T(8,128)}) custom-call(s32[2,16]{1,0:T(2,128)} %pad_add_fusion.info, bf16[16,16,128]{2,1,0:T(8,128)(2,1)} %bitcast.20, bf16[16,128,16,128]{3,2,1,0:T(8,128)(2,1)} %k_ref.1, bf16[16,128,16,128]{3,2,1,0:T(8,128)(2,1)} %v_ref.1), custom_call_target="tpu_custom_call" | custom-call | tf_op jit(solution)/shard_map/attend/pallas_call | solution.py:380
  36.3 1.6 %copy.27 = bf16[16,2,16,128]{3,0,1,2:T(8,128)(2,1)} copy(bf16[16,2,16,128]{3,2,1,0:T(8,128)(2,1)} %bitcast.22) | data formatting | bytes 262144 | tf_op jit(solution)/shard_map/reshape | solution.py:403
  37.9 1.8 %copy.26 = f32[16,2,16,128]{3,0,1,2:T(8,128)} copy(f32[16,2,16,128]{3,2,1,0:T(8,128)} %bitcast.21) | data formatting | bytes 524288 | tf_op jit(solution)/shard_map/reshape | solution.py:403
  39.7 54.1 %finish.1 = bf16[16,256]{1,0:T(8,128)(2,1)} custom-call(bf16[16,2,16,128]{3,2,1,0:T(8,128)(2,1)} %bitcast.19, f32[16,2,16,128]{3,2,1,0:T(8,128)} %bitcast.18, bf16[3,16,128]{2,1,0:T(8,128)(2,1)} %get-tuple-element.12.own_qkv, f32[1,16]{1,0:T(1,128)} %bitcast.25, f32[1,128]{1,0:T(1,128)} %bitcast.26, bf16[16,256]{1,0:T(8,128)(2,1)} %tokens.3, ...), custom_call_target="tpu_custom_call" | custom-call | tf_op jit(solution)/shard_map/finish/pallas_call | solution.py:405
  93.8 1.3 %copy.30 = bf16[16,256]{1,0:T(8,128)(2,1)} copy(bf16[16,256]{1,0:T(8,128)(2,1)} %finish.1) | data formatting | bytes 16384

commit v2 on v1

--- a/solution.py
+++ b/solution.py
@@ -48,6 +48,22 @@
     )
 
 
+def diagonal(seqs):
+    lane = lax.broadcasted_iota(jnp.int32, (seqs, LANES), 1)
+    return lane == lax.broadcasted_iota(jnp.int32, (seqs, LANES), 0)
+
+
+def to_lanes(column):
+    seqs = column.shape[0]
+    spread = jnp.where(diagonal(seqs), jnp.broadcast_to(column, (seqs, LANES)), 0.0)
+    return jnp.broadcast_to(jnp.sum(spread, axis=0, keepdims=True), (8, LANES))
+
+
+def to_rows(row, seqs):
+    spread = jnp.where(diagonal(seqs), jnp.broadcast_to(row, (seqs, LANES)), 0.0)
+    return jnp.sum(spread, axis=1, keepdims=True)
+
+
 def each_owner(n, owners, me, body):
     for i in range(owners):
         if owners == n:
@@ -67,20 +83,24 @@
 
 def project_kernel(
     n, heads, width, tokens, gain, wq, wk, wv, q_out, own_out,
-    sbuf, rbuf, gsrc, gbuf, send, recv,
+    wbuf, sbuf, rbuf, nsrc, ndst, gsrc, gbuf, send, recv, load,
 ):
     me = lax.axis_index("kv")
     barrier, count = greet(n, me)
+    loads = [
+        pltpu.make_async_copy(w, wbuf.at[j], load.at[j]) for j, w in enumerate((wq, wk, wv))
+    ]
+    for copy in loads:
+        copy.start()
     tokens_f = tokens[...].astype(F32)
     scaled = (tokens_f * gain[...]).astype(BF16)
     squares = jnp.sum(tokens_f * tokens_f, axis=1, keepdims=True)
-    squares = jnp.broadcast_to(squares, (tokens.shape[0], LANES))
-    for j, w in enumerate((wq, wk, wv)):
-        part = jnp.dot(scaled, w[...], preferred_element_type=F32)
+    nsrc[...] = to_lanes(squares)
+    for j, copy in enumerate(loads):
+        copy.wait()
+        part = jnp.dot(scaled, wbuf[j], preferred_element_type=F32).astype(BF16)
         for h in range(heads):
             sbuf[h, j] = part[:, h * LANES : (h + 1) * LANES]
-    for h in range(heads):
-        sbuf[h, 3] = squares
     pl.semaphore_wait(barrier, count)
 
     def reduce_copy(o):
@@ -89,16 +109,27 @@
     def gather_copy(o):
         return remote(gsrc, gbuf.at[me], send.at[1, o], recv.at[1, me], {"kv": o})
 
-    each_owner(n, heads, me, lambda o: reduce_copy(o).start())
+    def norm_copy(o):
+        return remote(nsrc, ndst.at[me], send.at[2, o], recv.at[2, me], {"kv": o})
+
+    def start_parts(o):
+        norm_copy(o).start()
+        reduce_copy(o).start()
+
+    each_owner(n, heads, me, start_parts)
 
     def own():
         rbuf[me] = sbuf[me]
-        for i in range(1, n):
+        ndst[me] = nsrc[...]
+        for i in range(1, n):
+            landed(ndst, recv.at[2], lax.rem(me + n - i, n))
             landed(rbuf, recv.at[0], lax.rem(me + n - i, n))
-        total = rbuf[0]
+        total = rbuf[0].astype(F32)
+        norm = ndst[0]
         for k in range(1, n):
-            total = total + rbuf[k]
-        inverse = lax.rsqrt(total[3] / width + EPS)
+            total = total + rbuf[k].astype(F32)
+            norm = norm + ndst[k]
+        inverse = lax.rsqrt(to_rows(norm[:1], tokens.shape[0]) / width + EPS)
         for j in range(3):
             own_out[j] = (inverse * total[j]).astype(BF16)
         gsrc[...] = (inverse * total[0]).astype(BF16)
@@ -110,6 +141,7 @@
     each_owner(n, heads, me, lambda o: landed(gbuf, recv.at[1], o))
     q_out[...] = gbuf[...]
     each_owner(n, heads, me, lambda o: reduce_copy(o).wait_send())
+    each_owner(n, heads, me, lambda o: norm_copy(o).wait_send())
 
     def drain():
         for i in range(1, n):
@@ -121,7 +153,11 @@
 def attend_kernel(heads, scale, info, q_ref, k_ref, v_ref, value_out, lse_out):
     b = pl.program_id(0)
     live = info[1, b]
-    rows = 2 * heads
+    slot = lax.broadcasted_iota(jnp.int32, lse_out.shape, 1) == b
+
+    @pl.when(b == 0)
+    def _():
+        lse_out[...] = jnp.zeros_like(lse_out)
 
     @pl.when(live > 0)
     def _():
@@ -139,28 +175,30 @@
         )
         column = lax.broadcasted_iota(jnp.int32, scores.shape, 1)
         row = lax.broadcasted_iota(jnp.int32, scores.shape, 0)
-        visible = (lax.rem(column, heads) == lax.rem(row, heads)) & (column < live * heads)
+        if heads & (heads - 1) == 0:
+            same = ((column - row) & (heads - 1)) == 0
+        else:
+            same = lax.rem(column, heads) == lax.rem(row, heads)
+        visible = same & (column < live * heads)
         scores = jnp.where(visible, scores * scale, FLOOR_SCORE)
         peak = jnp.max(scores, axis=1, keepdims=True)
-        weights = jnp.where(visible, jnp.exp(scores - peak), 0.0)
+        weights = jnp.exp(scores - peak)
         totals = jnp.sum(weights, axis=1, keepdims=True)
-        position = lax.broadcasted_iota(jnp.int32, values.shape, 0)
-        values = jnp.where(position < live * heads, values, jnp.zeros_like(values))
         summed = jnp.dot(weights.astype(BF16), values, preferred_element_type=F32)
         value_out[0] = (summed / totals).astype(BF16)
-        lse_out[0] = jnp.broadcast_to(peak + jnp.log(totals), (rows, LANES))
+        lse_out[...] = jnp.where(slot, peak + jnp.log(totals), lse_out[...])
 
     @pl.when(live <= 0)
     def _():
         value_out[0] = jnp.zeros(value_out.shape[1:], BF16)
-        lse_out[0] = jnp.full((rows, LANES), FLOOR_SCORE, F32)
+        lse_out[...] = jnp.where(slot, FLOOR_SCORE, lse_out[...])
 
 
 def finish_kernel(
     n, team, heads, owners, tile, width, scale,
     vals, lses, own_qkv, mix, head_gain, tokens, mixer_gain, w_out, w_gate, w_up, w_down,
     out,
-    wo, wg, wu, wd, rvals, rlses, asrc, agat, xsrc, xdst, ssrc, sdst,
+    wo, wg, wu, wd, rvals, lsrc, rlses, asrc, agat, xsrc, xdst, ssrc, sdst,
     gsrc, gdst, hsrc, hgat, ysrc, ydst, send, recv, tsend, trecv, load,
 ):
     me = lax.axis_index("kv")
@@ -182,13 +220,20 @@
             w[:, pl.ds(hidden_width, padded - hidden_width)] = jnp.zeros(
                 (w.shape[0], padded - hidden_width), BF16
             )
+    seqs = tokens.shape[0]
+    first = lax.broadcasted_iota(jnp.int32, (8, LANES), 0) == 0
+    for h in range(heads):
+        rows = [
+            jnp.broadcast_to(lses[pl.ds(m * heads + h, 1), :], (8, LANES)) for m in range(2)
+        ]
+        lsrc[h] = jnp.where(first, rows[0], rows[1])
     pl.semaphore_wait(barrier, count)
 
     def vals_copy(o):
         return remote(vals.at[o], rvals.at[me], send.at[0, o], recv.at[0, me], {"kv": o})
 
     def lses_copy(o):
-        return remote(lses.at[o], rlses.at[me], send.at[1, o], recv.at[1, me], {"kv": o})
+        return remote(lsrc.at[o], rlses.at[me], send.at[1, o], recv.at[1, me], {"kv": o})
 
     def attended_copy(o):
         return remote(asrc, agat.at[me], send.at[2, o], recv.at[2, me], {"kv": o})
@@ -201,7 +246,7 @@
 
     def own_head():
         rvals[me] = vals[me]
-        rlses[me] = lses[me]
+        rlses[me] = lsrc[me]
         q, k, v = (own_qkv[j].astype(F32) for j in range(3))
         product = q * k
         lane = lax.broadcasted_iota(jnp.int32, product.shape, 1)
@@ -217,13 +262,16 @@
         for m in range(2):
             own_score = jnp.broadcast_to(own_scores[m], v.shape)
             peak = own_score
-            for j in range(n):
-                peak = jnp.maximum(peak, rlses[j, m])
+            parts = [
+                jnp.broadcast_to(to_rows(rlses[j][m : m + 1], seqs), v.shape) for j in range(n)
+            ]
+            for part in parts:
+                peak = jnp.maximum(peak, part)
             own_weight = jnp.exp(own_score - peak)
             totals = own_weight
             summed = own_weight.astype(BF16).astype(F32) * v
             for j in range(n):
-                weight = jnp.exp(rlses[j, m] - peak)
+                weight = jnp.exp(parts[j] - peak)
                 totals = totals + weight
                 summed = summed + weight * rvals[j, m].astype(F32)
             normed.append(summed / totals)
@@ -260,7 +308,7 @@
     residual_f = residual.astype(F32)
     scaled_mix = (residual_f * mixer_gain[...]).astype(BF16)
     squares = jnp.sum(residual_f * residual_f, axis=1, keepdims=True)
-    ssrc[...] = jnp.broadcast_to(squares, ssrc.shape)
+    ssrc[...] = to_lanes(squares)
 
     def squares_copy(o):
         return remote(ssrc, sdst.at[me], send.at[3, o], recv.at[3, me], {"kv": o})
@@ -292,7 +340,7 @@
         total = sdst[0]
         for j in range(1, n):
             total = total + sdst[j]
-        inverse = lax.rsqrt(total[:, :1] / width + EPS)
+        inverse = lax.rsqrt(to_rows(total[:1], seqs) / width + EPS)
         gate = gdst[0, 0].astype(F32)
         up = gdst[0, 1].astype(F32)
         for j in range(1, n):
@@ -353,15 +401,19 @@
             jax.ShapeDtypeStruct((heads, seqs, LANES), BF16),
             jax.ShapeDtypeStruct((3, seqs, LANES), BF16),
         ),
-        in_specs=[VMEM] * 5,
+        in_specs=[VMEM, VMEM, ANY, ANY, ANY],
         out_specs=(VMEM, VMEM),
         scratch_shapes=[
-            pltpu.VMEM((heads, 4, seqs, LANES), F32),
-            pltpu.VMEM((n, 4, seqs, LANES), F32),
+            pltpu.VMEM((3, *w_query.shape), BF16),
+            pltpu.VMEM((heads, 3, seqs, LANES), BF16),
+            pltpu.VMEM((n, 3, seqs, LANES), BF16),
+            pltpu.VMEM((8, LANES), F32),
+            pltpu.VMEM((n, 8, LANES), F32),
             pltpu.VMEM((seqs, LANES), BF16),
             pltpu.VMEM((heads, seqs, LANES), BF16),
-            pltpu.SemaphoreType.DMA((2, n)),
-            pltpu.SemaphoreType.DMA((2, n)),
+            pltpu.SemaphoreType.DMA((3, n)),
+            pltpu.SemaphoreType.DMA((3, n)),
+            pltpu.SemaphoreType.DMA((3,)),
         ],
         compiler_params=remote_params(collective_id=0),
         name="project",
@@ -381,7 +433,7 @@
         functools.partial(attend_kernel, heads, scale),
         out_shape=(
             jax.ShapeDtypeStruct((seqs, 2 * heads, LANES), BF16),
-            jax.ShapeDtypeStruct((seqs, 2 * heads, LANES), F32),
+            jax.ShapeDtypeStruct((2 * heads, LANES), F32),
         ),
         grid_spec=pltpu.PrefetchScalarGridSpec(
             num_scalar_prefetch=1,
@@ -391,7 +443,7 @@
                 cache_spec,
                 cache_spec,
             ],
-            out_specs=(part_spec, part_spec),
+            out_specs=(part_spec, pl.BlockSpec((2 * heads, LANES), lambda b, info: (0, 0))),
         ),
         compiler_params=pltpu.CompilerParams(
             dimension_semantics=("arbitrary",), vmem_limit_bytes=60 * 2**20
@@ -413,13 +465,14 @@
             pltpu.VMEM((span_width, owners * tile), BF16),
             pltpu.VMEM(w_down.shape, BF16),
             pltpu.VMEM((n, 2, seqs, LANES), BF16),
-            pltpu.VMEM((n, 2, seqs, LANES), F32),
+            pltpu.VMEM((heads, 8, LANES), F32),
+            pltpu.VMEM((n, 8, LANES), F32),
             pltpu.VMEM((seqs, LANES), BF16),
             pltpu.VMEM((heads, seqs, LANES), BF16),
             pltpu.VMEM((seqs, span_width), BF16),
             pltpu.VMEM((team, seqs, span_width), BF16),
-            pltpu.VMEM((seqs, LANES), F32),
-            pltpu.VMEM((n, seqs, LANES), F32),
+            pltpu.VMEM((8, LANES), F32),
+            pltpu.VMEM((n, 8, LANES), F32),
             pltpu.VMEM((owners, 2, seqs, tile), BF16),
             pltpu.VMEM((n, 2, seqs, tile), BF16),
             pltpu.VMEM((seqs, tile), BF16),
@@ -435,7 +488,7 @@
         compiler_params=remote_params(collective_id=1),
         name="finish",
     )(
-        by_head(values), by_head(lses), own_qkv, mix_weight[None], head_gain[None],
+        by_head(values), lses, own_qkv, mix_weight[None], head_gain[None],
         tokens, mixer_gain[None], w_out, w_gate, w_up, w_down,
     )
 

time: 95.8 us -> 81.8 us (0.85)
  Pallas kernels: 86.9 us -> 74.7 us
  local copies, waits for them, and re-layouts: 6.18 us -> 4.37 us
    pallas_call x1, Pallas kernels: 23.5 us -> 16.9 us  [local(): pl.pallas_call(functools.partial(project_kernel, n, heads, width), out_sh...]
    pallas_call x1, Pallas kernels: 54.1 us -> 48.3 us  [local(): pl.pallas_call(functools.partial(finish_kernel, n, team, heads, owners, t...]
    reshape x2 -> x1, local copies, waits for them, and re-layouts: 3.41 us -> 1.59 us  [by_head(): return array.reshape(seqs, 2, heads, LANES).transpose(2, 1, 0, 3)]
where the time goes in v2:
time: 81.8 us; the launch traced here: 81.1 us
  Pallas kernels  74.7 us (91%)
  local copies, waits for them, and re-layouts  4.37 us (5%)
  other arithmetic  2.01 us (2%)
    pallas_call x1, Pallas kernels, local(): pl.pallas_call(functools.partial(finish_kernel, n, team, heads, owners, t...  48.3 us
    pallas_call x1, Pallas kernels, local(): pl.pallas_call(functools.partial(project_kernel, n, heads, width), out_sh...  16.9 us
    pallas_call x1, Pallas kernels, local(): pl.pallas_call(functools.partial(attend_kernel, heads, scale), out_shape=...  9.49 us

profile of v2, /device:TPU:25, one launch (start us, length us, event | category | flops | bytes accessed | tf_op | source)
XLA Modules:
  0.0 81.1 jit_solution(9683180252081855784)
XLA Ops:
  0.0 0.7 subtract_bitcast_fusion
  0.7 0.7 subtract_compare_fusion
  1.3 0.1 select_reduce_fusion
  1.4 0.6 pad_add_fusion.info
  2.0 16.9 %project.1 = (bf16[16,16,128]{2,1,0:T(8,128)(2,1)}, bf16[3,16,128]{2,1,0:T(8,128)(2,1)}) custom-call(bf16[16,256]{1,0:T(8,128)(2,1)} %tokens.3, f32[1,256]{1,0:T(1,128)} %bitcast.17, bf16[256,2048]{1,0:T(8,128)(2,1)} %wq.1, bf16[256,2048]{1,0:T(8,128)(2,1)} %wk.1, bf16[256,2048]{1,0:T(8,128)(2,1)} %wv.1), custom_call_target="tpu_custom_call" | custom-call | tf_op jit(solution)/shard_map/project/pallas_call | solution.py:398
  19.0 1.5 %copy.24 = bf16[16,16,128]{2,0,1:T(8,128)(2,1)} copy(bf16[16,16,128]{2,1,0:T(8,128)(2,1)} %get-tuple-element.9) | data formatting | bytes 131072 | tf_op jit(solution)/shard_map/project/pallas_call | solution.py:398
  20.4 9.5 %attend.1 = (bf16[16,32,128]{2,1,0:T(8,128)(2,1)}, f32[32,128]{1,0:T(8,128)}) custom-call(s32[2,16]{1,0:T(2,128)} %pad_add_fusion.info, bf16[16,16,128]{2,1,0:T(8,128)(2,1)} %bitcast.15, bf16[16,128,16,128]{3,2,1,0:T(8,128)(2,1)} %k_ref.1, bf16[16,128,16,128]{3,2,1,0:T(8,128)(2,1)} %v_ref.1), custom_call_target="tpu_custom_call" | custom-call | tf_op jit(solution)/shard_map/attend/pallas_call | solution.py:432
  29.9 1.6 %copy.23 = bf16[16,2,16,128]{3,0,1,2:T(8,128)(2,1)} copy(bf16[16,2,16,128]{3,2,1,0:T(8,128)(2,1)} %bitcast.16) | data formatting | bytes 262144 | tf_op jit(solution)/shard_map/reshape | solution.py:455
  31.5 48.3 %finish.1 = bf16[16,256]{1,0:T(8,128)(2,1)} custom-call(bf16[16,2,16,128]{3,2,1,0:T(8,128)(2,1)} %bitcast.14, f32[32,128]{1,0:T(8,128)} %get-tuple-element.11.lses, bf16[3,16,128]{2,1,0:T(8,128)(2,1)} %get-tuple-element.12.own_qkv, f32[1,16]{1,0:T(1,128)} %bitcast.19, f32[1,128]{1,0:T(1,128)} %bitcast.20, bf16[16,256]{1,0:T(8,128)(2,1)} %tokens.3, ...), custom_call_target="tpu_custom_call" | custom-call | tf_op jit(solution)/shard_map/finish/pallas_call | solution.py:457
  79.8 1.3 %copy.26 = bf16[16,256]{1,0:T(8,128)(2,1)} copy(bf16[16,256]{1,0:T(8,128)(2,1)} %finish.1) | data formatting | bytes 16384
